TPU v7x, 32 devices: a whole 2x2x4 slice. The times are simulated.
32 devices in a mesh: sp: 16 (over z, y, x), tp: 2 (over core).
Axes of the slice: x: 2, y: 2, z: 4, core: 2. Of those that a mesh axis runs over, the one named last changes fastest.
Arguments:
- tokens: bfloat16 [16384, 2048], P('sp', 'tp'), may hold values from -6 to 6
- norm_gain: float32 [2048], replicated, may hold values from 0.1 to 1.9
- w_query: bfloat16 [2048, 1024], P('sp', 'tp'), may hold values from -0.125 to 0.125
- w_key: bfloat16 [2048, 512], P('sp', 'tp'), may hold values from -0.125 to 0.125
- w_value: bfloat16 [2048, 512], P('sp', 'tp'), may hold values from -0.125 to 0.125
- w_glu_a: bfloat16 [2048, 1024], P('sp', 'tp'), may hold values from -0.125 to 0.125
- w_glu_b: bfloat16 [2048, 1024], P('sp', 'tp'), may hold values from -0.125 to 0.125
- q_gain: float32 [64], replicated, may hold values from 0.8 to 7
- k_gain: float32 [64], replicated, may hold values from 0.8 to 7
- sink_logit: float32 [16], P('tp'), may hold values from 1 to 4
- conv_taps: float32 [31, 1024], P(None, 'tp'), may hold values from -1 to 1
- chan_gain: float32 [1024], P('tp'), may hold values from 0.1 to 1.9
- chan_bias: float32 [1024], P('tp'), may hold values from -3 to 3
- w_attn_back: bfloat16 [2048, 1024], P('sp', 'tp'), may hold values from -0.1875 to 0.1875
- w_conv_back: bfloat16 [2048, 1024], P('sp', 'tp'), may hold values from -0.1875 to 0.1875
Outputs:
- mixed: bfloat16 [16384, 2048], P(('sp', 'tp'))
- log_weight: float32 [16, 16384], P('tp', 'sp')
All inputs are finite; a program needn't handle non-finite values.
Results may differ from a plain program's by a relative error of at most 0.014.
The roundings to bfloat16 on the way count: a program that leaves them out, or rounds other values in their place, can miss the bound.
Values may be sent and summed in bfloat16 or wider, within the bound.
A program may use at most 128 MiB of HBM per device.

v0:
```python
import jax
import jax.numpy as jnp
from jax import lax
from jax.sharding import PartitionSpec as P

HEAD = 64
CH = 1024
KW = 31
WINDOW = 128
EPS = 1e-06


def passed_along(value, axis, steps):
    count = lax.axis_size(axis)
    leading, last = (max(0, -steps), min(count, count - steps))
    return lax.ppermute(value, axis, [(source, source + steps) for source in range(leading, last)])


def row_norm(inputs, scale_vec):
    squares = jnp.mean(inputs * inputs, axis=-1, keepdims=True)
    return inputs * lax.rsqrt(squares + EPS) * scale_vec


def local(
    tokens,
    norm_gain,
    w_query,
    w_key,
    w_value,
    w_glu_a,
    w_glu_b,
    q_gain,
    k_gain,
    sink_logit,
    conv_taps,
    chan_gain,
    chan_bias,
    w_attn_back,
    w_conv_back,
):
    row_count = tokens.shape[0]
    q_local = w_query.shape[1] // HEAD
    kv_local = w_key.shape[1] // HEAD
    group_size = q_local // kv_local
    kv_width = kv_local * HEAD
    gathered = lax.all_gather(tokens, "tp", axis=1, tiled=True)
    normed = row_norm(gathered.astype(jnp.float32), norm_gain).astype(jnp.bfloat16)
    whole_rows = (
        lax.all_gather(w_query, "sp", axis=0, tiled=True),
        lax.all_gather(w_key, "sp", axis=0, tiled=True),
        lax.all_gather(w_value, "sp", axis=0, tiled=True),
        lax.all_gather(w_glu_a, "sp", axis=0, tiled=True),
        lax.all_gather(w_glu_b, "sp", axis=0, tiled=True),
        lax.all_gather(w_attn_back, "sp", axis=0, tiled=True),
        lax.all_gather(w_conv_back, "sp", axis=0, tiled=True),
    )
    projected = tuple(
        (jnp.dot(normed, weight, preferred_element_type=jnp.float32) for weight in whole_rows[:5])
    )
    attn_back = whole_rows[5]
    conv_back = whole_rows[6]
    query_raw, key_raw, value_raw, glu_a, glu_b = projected
    queries = row_norm(query_raw.reshape(row_count, q_local, HEAD), q_gain).astype(jnp.bfloat16)
    key_rows = (
        row_norm(key_raw.reshape(row_count, kv_local, HEAD), k_gain)
        .astype(jnp.bfloat16)
        .reshape(row_count, kv_width)
    )
    value_rows = value_raw.astype(jnp.bfloat16)
    gated_rows = (glu_a * jax.nn.sigmoid(glu_b)).astype(jnp.bfloat16)
    key_value = jnp.concatenate([key_rows, value_rows], 1)
    key_value_rim = passed_along(key_value[row_count - WINDOW :], "sp", 1)
    gated_rim = passed_along(gated_rows[row_count - (KW - 1) :], "sp", 1)
    block_count = row_count // WINDOW
    extended = jnp.concatenate([key_value_rim, key_value], 0).reshape(
        block_count + 1, WINDOW, 2 * kv_width
    )
    band = jnp.concatenate([extended[:-1], extended[1:]], 1)
    key_band = band[:, :, :kv_width].reshape(block_count, 2 * WINDOW, kv_local, HEAD)
    value_band = band[:, :, kv_width:].reshape(block_count, 2 * WINDOW, kv_local, HEAD)
    grouped = queries.reshape(block_count, WINDOW, kv_local, group_size, HEAD)
    scores = jnp.einsum(
        "nqhgd,nkhd->nhgqk", grouped, key_band, preferred_element_type=jnp.float32
    ) * HEAD ** (-0.5)
    offsets = jnp.arange(WINDOW, dtype=jnp.int32)
    band_offsets = jnp.arange(2 * WINDOW, dtype=jnp.int32)
    distance = WINDOW + offsets[:, None] - band_offsets[None, :]
    allowed = (distance >= 0) & (distance < WINDOW)
    anchor = lax.axis_index("sp") * row_count
    key_position = (
        anchor
        + jnp.arange(block_count, dtype=jnp.int32)[:, None] * WINDOW
        - WINDOW
        + band_offsets[None, :]
    )
    visible = (allowed[None, :, :] & (key_position[:, None, :] >= 0))[:, None, None]
    sink_table = sink_logit.reshape(kv_local, group_size)[None, :, :, None, None]
    masked = jnp.where(visible, scores, -jnp.inf)
    largest = jnp.maximum(jnp.max(masked, axis=-1, keepdims=True), sink_table)
    weights = jnp.where(visible, jnp.exp(scores - largest), 0.0)
    weight_sum = jnp.sum(weights, axis=-1, keepdims=True) + jnp.exp(sink_table - largest)
    log_weight = (largest + jnp.log(weight_sum))[..., 0]
    log_weight = jnp.transpose(log_weight, (1, 2, 0, 3)).reshape(q_local, row_count)
    probabilities = (weights / weight_sum).astype(jnp.bfloat16)
    attended = jnp.einsum(
        "nhgqk,nkhd->nqhgd", probabilities, value_band, preferred_element_type=jnp.float32
    )
    attended = attended.astype(jnp.bfloat16).reshape(row_count, q_local * HEAD)
    gate_extended = jnp.concatenate([gated_rim, gated_rows], 0).astype(jnp.float32)
    convolved = jnp.zeros((row_count, gated_rows.shape[1]), jnp.float32)
    for tap_index in range(KW):
        convolved = (
            convolved + conv_taps[tap_index] * gate_extended[tap_index : tap_index + row_count]
        )
    channel_sums = lax.psum(
        (jnp.sum(convolved, axis=1), jnp.sum(convolved * convolved, axis=1)), "tp"
    )
    center = (channel_sums[0] / CH)[:, None]
    spread = (channel_sums[1] / CH)[:, None] - center * center
    conv_rows = jax.nn.silu(
        (convolved - center) * lax.rsqrt(spread + EPS) * chan_gain + chan_bias
    ).astype(jnp.bfloat16)
    contract = (((1,), (1,)), ((), ()))
    result = lax.dot_general(attended, attn_back, contract, preferred_element_type=jnp.float32)
    summed = lax.psum_scatter(
        (
            result
            + lax.dot_general(conv_rows, conv_back, contract, preferred_element_type=jnp.float32)
        ).astype(jnp.bfloat16),
        "tp",
        scatter_dimension=0,
        tiled=True,
    )
    return (summed, log_weight)


def solution(mesh):
    placed = (
        P("sp", "tp"),
        P(),
        P("sp", "tp"),
        P("sp", "tp"),
        P("sp", "tp"),
        P("sp", "tp"),
        P("sp", "tp"),
        P(),
        P(),
        P("tp"),
        P(None, "tp"),
        P("tp"),
        P("tp"),
        P("sp", "tp"),
        P("sp", "tp"),
    )
    return jax.shard_map(
        local,
        mesh=mesh,
        in_specs=placed,
        out_specs=(P(("sp", "tp"), None), P("tp", "sp")),
        check_vma=False,
    )
```

profile of v0, /device:TPU:0, one launch (start us, length us, event | category | flops | bytes accessed | tf_op | source)
XLA Modules:
  0.0 476.1 jit_solution(15516827644429883974)
XLA Ops:
  7.2 0.7 all-gather.9.cloned.1.call-update
  8.0 0.7 all-gather.15.cloned.1.call-update
  8.7 0.7 all-gather.11.cloned.1.call-update
  11.2 0.7 all-gather.17.cloned.1.call-update
  11.9 0.7 all-gather.23.cloned.1.call-update
  14.7 11.3 %all-gather.9.cloned.1.call-done = bf16[1024,2048]{1,0:T(8,128)(2,1)} async-done(((bf16[1024,1024]{1,0:T(8,128)(2,1)}), bf16[1024,2048]{1,0:T(8,128)(2,1)}) %all-gather.9.cloned.1.call-update) | async-done | bytes 4194320 | tf_op jit(solution)/shard_map/all_gather | solution.py:46
  26.0 3.1 fusion
  29.1 61.3 %all-gather.15.cloned.1.call-done = bf16[2048,512]{1,0:T(8,128)(2,1)} async-done(((bf16[128,512]{1,0:T(8,128)(2,1)}), bf16[2048,512]{1,0:T(8,128)(2,1)}) %all-gather.15.cloned.1.call-update) | async-done | bytes 2097168 | tf_op jit(solution)/shard_map/all_gather | solution.py:49
  90.3 6.7 %bitcast_reduce_fusion = (f32[1024,8]{0,1:T(8,128)S(1)}, f32[1024,512]{0,1:T(8,128)}) fusion(bf16[2048,512]{1,0:T(8,128)(2,1)} %all-gather.15.cloned.1.call-done, bf16[1024,2048]{1,0:T(8,128)(2,1)} %all-gather.9.cloned.1.call-done, f32[2048]{0:T(1024)S(1)} %copy-done.28, f32[1024]{0:T(1024)S(1)} %add_rsqrt_fusion.3), kind=kOutput, calls=%fused_computation.75 | convolution fusion | flops 2156912640 | bytes 8433664 | tf_op jit(solution)/shard_map/dot_general | solution.py:58
  97.0 50.0 %all-gather.11.cloned.1.call-done = bf16[2048,256]{1,0:T(8,128)(2,1)} async-done(((bf16[128,256]{1,0:T(8,128)(2,1)}), bf16[2048,256]{1,0:T(8,128)(2,1)}) %all-gather.11.cloned.1.call-update) | async-done | bytes 1048592 | tf_op jit(solution)/shard_map/all_gather | solution.py:50
  147.0 4.0 bitcast_reduce_fusion.1
  151.1 57.8 %all-gather.19.cloned.1.call-done = bf16[2048,512]{1,0:T(8,128)(2,1)} async-done(((bf16[128,512]{1,0:T(8,128)(2,1)}), bf16[2048,512]{1,0:T(8,128)(2,1)}) %all-gather.19.cloned.1.call-update) | async-done | bytes 2097168 | tf_op jit(solution)/shard_map/all_gather | solution.py:52
  208.9 6.6 %fusion.69 = f32[1024,512]{1,0:T(8,128)} fusion(bf16[2048,512]{1,0:T(8,128)(2,1)} %all-gather.19.cloned.1.call-done, bf16[1024,2048]{1,0:T(8,128)(2,1)} %all-gather.9.cloned.1.call-done, f32[2048]{0:T(1024)S(1)} %copy-done.28, f32[1024]{0:T(1024)S(1)} %add_rsqrt_fusion.3), kind=kOutput, calls=%fused_computation.135 | convolution fusion | flops 2155872256 | bytes 8400896 | tf_op jit(solution)/shard_map/dot_general | solution.py:58
  215.5 55.2 %all-gather.21.cloned.1.call-done = bf16[2048,512]{1,0:T(8,128)(2,1)} async-done(((bf16[128,512]{1,0:T(8,128)(2,1)}), bf16[2048,512]{1,0:T(8,128)(2,1)}) %all-gather.21.cloned.1.call-update) | async-done | bytes 2097168 | tf_op jit(solution)/shard_map/all_gather | solution.py:53
  270.7 6.1 %multiply_convert_fusion.1 = bf16[1024,512]{1,0:T(8,128)(2,1)S(1)} fusion(f32[1024,512]{1,0:T(8,128)} %fusion.69, bf16[2048,512]{1,0:T(8,128)(2,1)} %all-gather.21.cloned.1.call-done, bf16[1024,2048]{1,0:T(8,128)(2,1)} %all-gather.9.cloned.1.call-done, f32[2048]{0:T(1024)S(1)} %copy-done.28, f32[1024]{0:T(1024)S(1)} %add_rsqrt_fusion.3), kind=kOutput, calls=%fused_computation.81 | convolution fusion | flops 2158493696 | bytes 9449472 | tf_op jit(solution)/shard_map/dot_general | solution.py:58
  276.8 3.4 collective-permute-start.1
  280.4 46.8 %all-gather.13.cloned.1.call-done = bf16[2048,256]{1,0:T(8,128)(2,1)} async-done(((bf16[128,256]{1,0:T(8,128)(2,1)}), bf16[2048,256]{1,0:T(8,128)(2,1)}) %all-gather.13.cloned.1.call-update) | async-done | bytes 1048592 | tf_op jit(solution)/shard_map/all_gather | solution.py:51
  327.2 4.2 convolution_convert_fusion
  331.4 0.7 fusion.58
  332.8 4.0 collective-permute-start
  337.3 9.5 %fusion.76 = (f32[1024]{0:T(1024)S(1)}, f32[1024]{0:T(1024)S(1)}, f32[1024,512]{1,0:T(8,128)}) fusion(f32[1054,512]{1,0:T(8,128)S(1)} %maximum_convert_fusion, f32[512]{0:T(512)S(1)} %bitcast.141, f32[512]{0:T(512)S(1)} %bitcast.142, f32[512]{0:T(512)S(1)} %bitcast.144, f32[512]{0:T(512)S(1)} %bitcast.145, f32[512]{0:T(512)S(1)} %bitcast.146, ...), kind=kLoop, calls=%fused_computation.138 | loop fusion | flops 33552384 | bytes 67180544 | tf_op jit(solution)/shard_map/reduce_sum | solution.py:116
  346.8 2.5 all-reduce
  349.3 1.3 fusion.42
  352.3 1.9 fusion.3
  354.3 2.2 fusion.6
  356.7 2.4 fusion.41
  359.1 0.7 copy.46
  359.8 29.5 %all-gather.17.cloned.1.call-done = bf16[2048,512]{1,0:T(8,128)(2,1)} async-done(((bf16[128,512]{1,0:T(8,128)(2,1)}), bf16[2048,512]{1,0:T(8,128)(2,1)}) %all-gather.17.cloned.1.call-update) | async-done | bytes 2097168 | tf_op jit(solution)/shard_map/all_gather | solution.py:54
  389.3 7.4 %fusion.45 = f32[1024,2048]{1,0:T(8,128)} fusion(bf16[2048,512]{1,0:T(8,128)(2,1)} %all-gather.17.cloned.1.call-done, bf16[64,8,8,128]{3,2,1,0:T(8,128)(2,1)S(1)} %bitcast.127), kind=kOutput, calls=%fused_computation.91 | convolution fusion | flops 2147483648 | bytes 11534336 | tf_op jit(solution)/shard_map/dot_general | solution.py:124
  396.7 54.6 %all-gather.23.cloned.1.call-done = bf16[2048,512]{1,0:T(8,128)(2,1)} async-done(((bf16[128,512]{1,0:T(8,128)(2,1)}), bf16[2048,512]{1,0:T(8,128)(2,1)}) %all-gather.23.cloned.1.call-update) | async-done | bytes 2097168 | tf_op jit(solution)/shard_map/all_gather | solution.py:55
  451.2 7.3 %add_convert_fusion = bf16[1024,2048]{1,0:T(8,128)(2,1)} fusion(f32[1024,2048]{1,0:T(8,128)} %fusion.45, bf16[2048,512]{1,0:T(8,128)(2,1)} %all-gather.23.cloned.1.call-done, f32[1024,512]{1,0:T(8,128)S(1)} %copy-done, f32[512]{0:T(512)S(1)} %copy-done.29, f32[512]{0:T(512)S(1)} %copy-done.30, f32[1024]{0:T(1024)S(1)} %get-tuple-element.43, ...), kind=kOutput, calls=%fused_computation.10 | convolution fusion | flops 2156396544 | bytes 16789504 | tf_op jit(solution)/shard_map/dot_general | solution.py:128
  459.3 10.3 %reduce-scatter.2.cloned.1.call-done = bf16[512,2048]{1,0:T(8,128)(2,1)} async-done(((bf16[1024,2048]{1,0:T(8,128)(2,1)}), bf16[512,2048]{1,0:T(8,128)(2,1)}) %reduce-scatter.2.cloned.1.call-update) | async-done | bytes 2097168 | tf_op jit(solution)/shard_map/reduce_scatter | solution.py:125
  (108 shorter events, 7.7 us)
Async XLA Ops:
  7.2 5.6 %copy-start.4 = (f32[31,512]{1,0:T(8,128)S(1)}, f32[31,512]{1,0:T(8,128)}, u32[]{:S(2)}) copy-start(f32[31,512]{1,0:T(8,128)} %param.25) | copy-start | bytes 190468
  7.2 6.9 %copy-start.26 = (f32[8]{0:T(128)S(1)}, f32[8]{0:T(128)}, u32[]{:S(2)}) copy-start(f32[8]{0:T(128)} %param.24) | copy-start | bytes 100
  7.2 7.0 %copy-start.27 = (f32[64]{0:T(128)S(1)}, f32[64]{0:T(128)}, u32[]{:S(2)}) copy-start(f32[64]{0:T(128)} %param.23) | copy-start | bytes 772
  7.2 18.8 %all-gather.9.cloned.1.call-start = ((), (), s32[]{:S(2)}) async-start(), calls=%async_computation.1 | async-start | bytes 6291456 | tf_op jit(solution)/shard_map/all_gather | solution.py:46
  7.9 82.4 %all-gather.15.cloned.1.call-start = ((), (), s32[]{:S(2)}) async-start(), calls=%async_computation.4 | async-start | bytes 2228224 | tf_op jit(solution)/shard_map/all_gather | solution.py:49
  8.7 138.3 %all-gather.11.cloned.1.call-start = ((), (), s32[]{:S(2)}) async-start(), calls=%async_computation.2 | async-start | bytes 1114112 | tf_op jit(solution)/shard_map/all_gather | solution.py:50
  9.4 199.5 %all-gather.19.cloned.1.call-start = ((), (), s32[]{:S(2)}) async-start(), calls=%async_computation.6 | async-start | bytes 2228224 | tf_op jit(solution)/shard_map/all_gather | solution.py:52
  10.0 260.7 %all-gather.21.cloned.1.call-start = ((), (), s32[]{:S(2)}) async-start(), calls=%async_computation.7 | async-start | bytes 2228224 | tf_op jit(solution)/shard_map/all_gather | solution.py:53
  10.6 316.7 %all-gather.13.cloned.1.call-start = ((), (), s32[]{:S(2)}) async-start(), calls=%async_computation.3 | async-start | bytes 1114112 | tf_op jit(solution)/shard_map/all_gather | solution.py:51
  11.2 378.1 %all-gather.17.cloned.1.call-start = ((), (), s32[]{:S(2)}) async-start(), calls=%async_computation.5 | async-start | bytes 2228224 | tf_op jit(solution)/shard_map/all_gather | solution.py:54
  11.9 439.3 %all-gather.23.cloned.1.call-start = ((), (), s32[]{:S(2)}) async-start(), calls=%async_computation.8 | async-start | bytes 2228224 | tf_op jit(solution)/shard_map/all_gather | solution.py:55
  12.7 457.0 %reduce-scatter.2.cloned.1.call-start = ((), (), s32[]{:S(2)}) async-start(), calls=%async_computation.9 | async-start | bytes 6291456 | tf_op jit(solution)/shard_map/reduce_scatter | solution.py:125
  14.6 75.7 %copy-start.28 = (f32[2048]{0:T(1024)S(1)}, f32[2048]{0:T(1024)}, u32[]{:S(2)}) copy-start(f32[2048]{0:T(1024)} %param.16) | copy-start | bytes 24580
  276.8 59.9 %collective-permute-start.1 = (bf16[30,512]{1,0:T(8,128)(2,1)S(1)}, bf16[30,512]{1,0:T(8,128)(2,1)S(1)}, u32[]{:S(2)}, u32[]{:S(2)}) collective-permute-start(bf16[30,512]{1,0:T(8,128)(2,1)S(1)} %slice.281), channel_id=1, source_target_pairs={{0,2},{2,4},{4,6},{6,8},{8,10},{10,12},{12,14},{14,16},{16,18},{18... | collective-permute-start | bytes 92168 | tf_op jit(solution)/shard_map/ppermute | solution.py:16
  327.2 4.9 %copy-start.1 = (f32[1024,512]{0,1:T(8,128)S(1)}, f32[1024,512]{0,1:T(8,128)}, u32[]{:S(2)}) copy-start(f32[1024,512]{0,1:T(8,128)} %get-tuple-element.47) | copy-start | bytes 6291460
  332.1 4.7 copy-start.3
  332.6 4.6 copy-start.5
  332.6 4.6 copy-start.6
  332.6 4.6 copy-start.7
  332.6 4.6 copy-start.8
  332.6 4.6 copy-start.9
  332.6 4.6 copy-start.10
  332.6 4.6 copy-start.11
  332.6 4.6 copy-start.12
  332.7 4.6 copy-start.13
  332.7 4.6 copy-start.14
  332.7 4.6 copy-start.15
  332.7 4.6 copy-start.16
  332.8 16.5 %collective-permute-start = (bf16[128,512]{0,1:T(8,128)(2,1)}, bf16[128,512]{0,1:T(8,128)(2,1)}, u32[]{:S(2)}, u32[]{:S(2)}) collective-permute-start(bf16[128,512]{0,1:T(8,128)(2,1)} %fusion.58), channel_id=1, source_target_pairs={{0,2},{2,4},{4,6},{6,8},{8,10},{10,12},{12,14},{14,16},{16,18},{18... | collective-permute-start | bytes 393224 | tf_op jit(solution)/shard_map/ppermute | solution.py:16
  389.3 62.0 %copy-start = (f32[1024,512]{1,0:T(8,128)S(1)}, f32[1024,512]{1,0:T(8,128)}, u32[]{:S(2)}) copy-start(f32[1024,512]{1,0:T(8,128)} %get-tuple-element.6) | copy-start | bytes 6291460
  389.3 62.0 %copy-start.29 = (f32[512]{0:T(512)S(1)}, f32[512]{0:T(512)}, u32[]{:S(2)}) copy-start(f32[512]{0:T(512)} %param.27) | copy-start | bytes 6148
  389.3 62.0 %copy-start.30 = (f32[512]{0:T(512)S(1)}, f32[512]{0:T(512)}, u32[]{:S(2)}) copy-start(f32[512]{0:T(512)} %param.26) | copy-start | bytes 6148
  (10 other events, 40.5 us)
Sparse Core Ops, SparseCore 0:
  9.5 16.3 all-gather.8
  28.7 61.5 all-gather.14
  93.1 53.8 all-gather.10
  149.6 59.2 all-gather.18
  211.5 59.1 all-gather.20
  273.3 53.8 all-gather.12
  330.0 59.2 all-gather.16
  392.0 59.1 all-gather.22
  458.7 10.8 reduce-scatter.1
where the time goes:
time: 476 us
  waiting for transfers between devices  382 us (80%)
  matrix products  46.7 us (10%)
  other arithmetic  18 us (4%)
  between operations  14.4 us (3%)
  starting transfers between devices  7.71 us (2%)
  local copies, waits for them, and re-layouts  5.14 us (1%)
    all_gather x1, waiting for transfers between devices, local(): lax.all_gather(w_query, 'sp', axis=0, tiled=True)  61.3 us
    all_gather x1, waiting for transfers between devices, local(): lax.all_gather(w_glu_a, 'sp', axis=0, tiled=True)  57.8 us
    all_gather x1, waiting for transfers between devices, local(): lax.all_gather(w_glu_b, 'sp', axis=0, tiled=True)  55.2 us
    all_gather x1, waiting for transfers between devices, local(): lax.all_gather(w_conv_back, 'sp', axis=0, tiled=True)  54.6 us
    all_gather x1, waiting for transfers between devices, local(): lax.all_gather(w_key, 'sp', axis=0, tiled=True)  50 us
    all_gather x1, waiting for transfers between devices, local(): lax.all_gather(w_value, 'sp', axis=0, tiled=True)  46.8 us
    all_gather x1, waiting for transfers between devices, local(): lax.all_gather(w_attn_back, 'sp', axis=0, tiled=True)  29.5 us
    dot_general x5, matrix products, local(): jnp.dot(normed, weight, preferred_element_type=jnp.float32)  27.6 us
  transfers between devices with their start and end apart: 11, of which 9 were waited for; matrix products, arithmetic and copies ran while one was open for 13% of the time, Pallas kernels for 0%

commit v1 on v0

--- a/solution.py
+++ b/solution.py
@@ -48,7 +48,9 @@
     whole_rows = (
         lax.all_gather(w_query, "sp", axis=0, tiled=True),
         lax.all_gather(w_key, "sp", axis=0, tiled=True),
-        lax.all_gather(w_value, "sp", axis=0, tiled=True),
+        jnp.concatenate(
+            lax.all_to_all(jnp.stack([w_value] * lax.axis_size("sp")), "sp", 0, 0), axis=0
+        ),
         lax.all_gather(w_glu_a, "sp", axis=0, tiled=True),
         lax.all_gather(w_glu_b, "sp", axis=0, tiled=True),
         lax.all_gather(w_attn_back, "sp", axis=0, tiled=True),

time: 476 us -> 420 us (0.88)
  waiting for transfers between devices: 382 us -> 316 us
  starting transfers between devices: 7.71 us -> 15.8 us
    all_gather x1 -> x0, waiting for transfers between devices: 46.8 us -> none  [local(): lax.all_gather(w_value, 'sp', axis=0, tiled=True)]
    all_gather x1, waiting for transfers between devices: 11.3 us -> 2.58 us  [local(): gathered = lax.all_gather(tokens, 'tp', axis=1, tiled=True)]
    all_to_all x0 -> x1, starting transfers between devices: none -> 8.34 us  [local(): lax.all_to_all(jnp.stack([w_value] * lax.axis_size('sp')), 'sp', 0, 0)]
    all_gather x1, waiting for transfers between devices: 29.5 us -> 23.1 us  [local(): lax.all_gather(w_attn_back, 'sp', axis=0, tiled=True)]
  transfers between devices with their start and end apart: 11 -> 11, of which waited for: 9 -> 8; matrix products, arithmetic and copies ran while one was open for 13% -> 15% of each run, Pallas kernels for 0% -> 0%
where the time goes in v1:
time: 420 us
  waiting for transfers between devices  316 us (75%)
  matrix products  46.3 us (11%)
  other arithmetic  18 us (4%)
  starting transfers between devices  15.8 us (4%)
  between operations  14.8 us (4%)
  local copies, waits for them, and re-layouts  7.23 us (2%)
    all_gather x1, waiting for transfers between devices, local(): lax.all_gather(w_glu_a, 'sp', axis=0, tiled=True)  61.5 us
    all_gather x1, waiting for transfers between devices, local(): lax.all_gather(w_query, 'sp', axis=0, tiled=True)  57.6 us
    all_gather x1, waiting for transfers between devices, local(): lax.all_gather(w_glu_b, 'sp', axis=0, tiled=True)  55.4 us
    all_gather x1, waiting for transfers between devices, local(): lax.all_gather(w_conv_back, 'sp', axis=0, tiled=True)  54.6 us
    all_gather x1, waiting for transfers between devices, local(): lax.all_gather(w_key, 'sp', axis=0, tiled=True)  46 us
    dot_general x5, matrix products, local(): jnp.dot(normed, weight, preferred_element_type=jnp.float32)  27.2 us
    all_gather x1, waiting for transfers between devices, local(): lax.all_gather(w_attn_back, 'sp', axis=0, tiled=True)  23.1 us
    reduce_scatter x1, waiting for transfers between devices, local(): lax.psum_scatter((result + lax.dot_general(conv_rows, conv_back, contract...  10.3 us
  transfers between devices with their start and end apart: 11, of which 8 were waited for; matrix products, arithmetic and copies ran while one was open for 15% of the time, Pallas kernels for 0%

profile of v1, /device:TPU:0, one launch (start us, length us, event | category | flops | bytes accessed | tf_op | source)
XLA Modules:
  0.0 420.1 jit_solution(7888146449241350972)
XLA Ops:
  7.2 0.7 all-gather.8.cloned.1.call-update
  8.0 0.7 all-gather.16.cloned.1.call-update
  8.7 0.7 all-gather.18.cloned.1.call-update
  11.2 1.1 stack.2
  12.2 8.3 %all-to-all-start = ((bf16[16,128,256]{2,1,0:T(8,128)(2,1)}), bf16[16,128,256]{2,1,0:T(8,128)(2,1)S(1)}, u32[]{:S(2)}, u32[]{:S(2)}) async-start(bf16[16,128,256]{2,1,0:T(8,128)(2,1)} %stack.2), calls=%async_computation | async-start | bytes 2097152 | tf_op jit(solution)/shard_map/all_to_all | solution.py:52
  20.6 0.7 all-gather.20.cloned.1.call-update
  23.4 2.6 all-gather.8.cloned.1.call-done
  25.9 3.1 fusion
  29.0 61.5 %all-gather.16.cloned.1.call-done = bf16[2048,512]{1,0:T(8,128)(2,1)} async-done(((bf16[128,512]{1,0:T(8,128)(2,1)}), bf16[2048,512]{1,0:T(8,128)(2,1)}) %all-gather.16.cloned.1.call-update) | async-done | bytes 2097168 | tf_op jit(solution)/shard_map/all_gather | solution.py:54
  90.6 6.6 %fusion.69 = f32[1024,512]{1,0:T(8,128)} fusion(bf16[2048,512]{1,0:T(8,128)(2,1)} %all-gather.16.cloned.1.call-done, bf16[1024,2048]{1,0:T(8,128)(2,1)} %all-gather.8.cloned.1.call-done, f32[2048]{0:T(1024)S(1)} %copy-done.30, f32[1024]{0:T(1024)S(1)} %add_rsqrt_fusion.3), kind=kOutput, calls=%fused_computation.135 | convolution fusion | flops 2155872256 | bytes 8400896 | tf_op jit(solution)/shard_map/dot_general | solution.py:60
  97.2 55.4 %all-gather.18.cloned.1.call-done = bf16[2048,512]{1,0:T(8,128)(2,1)} async-done(((bf16[128,512]{1,0:T(8,128)(2,1)}), bf16[2048,512]{1,0:T(8,128)(2,1)}) %all-gather.18.cloned.1.call-update) | async-done | bytes 2097168 | tf_op jit(solution)/shard_map/all_gather | solution.py:55
  152.6 6.1 %multiply_convert_fusion.1 = bf16[1024,512]{1,0:T(8,128)(2,1)S(1)} fusion(f32[1024,512]{1,0:T(8,128)} %fusion.69, bf16[2048,512]{1,0:T(8,128)(2,1)} %all-gather.18.cloned.1.call-done, bf16[1024,2048]{1,0:T(8,128)(2,1)} %all-gather.8.cloned.1.call-done, f32[2048]{0:T(1024)S(1)} %copy-done.30, f32[1024]{0:T(1024)S(1)} %add_rsqrt_fusion.3), kind=kOutput, calls=%fused_computation.81 | convolution fusion | flops 2158493696 | bytes 9449472 | tf_op jit(solution)/shard_map/dot_general | solution.py:60
  158.7 1.0 copy-done.2
  159.7 3.4 collective-permute-start.1
  163.1 46.0 %all-gather.10.cloned.1.call-done = bf16[2048,256]{1,0:T(8,128)(2,1)} async-done(((bf16[128,256]{1,0:T(8,128)(2,1)}), bf16[2048,256]{1,0:T(8,128)(2,1)}) %all-gather.10.cloned.1.call-update) | async-done | bytes 1048592 | tf_op jit(solution)/shard_map/all_gather | solution.py:50
  209.1 4.0 bitcast_reduce_fusion.1
  213.4 57.6 %all-gather.12.cloned.1.call-done = bf16[2048,512]{1,0:T(8,128)(2,1)} async-done(((bf16[128,512]{1,0:T(8,128)(2,1)}), bf16[2048,512]{1,0:T(8,128)(2,1)}) %all-gather.12.cloned.1.call-update) | async-done | bytes 2097168 | tf_op jit(solution)/shard_map/all_gather | solution.py:49
  271.0 6.7 %bitcast_reduce_fusion = (f32[1024,8]{0,1:T(8,128)S(1)}, f32[1024,512]{0,1:T(8,128)}) fusion(bf16[2048,512]{1,0:T(8,128)(2,1)} %all-gather.12.cloned.1.call-done, bf16[1024,2048]{1,0:T(8,128)(2,1)} %all-gather.8.cloned.1.call-done, f32[2048]{0:T(1024)S(1)} %copy-done.30, f32[1024]{0:T(1024)S(1)} %add_rsqrt_fusion.3), kind=kOutput, calls=%fused_computation.75 | convolution fusion | flops 2156912640 | bytes 8433664 | tf_op jit(solution)/shard_map/dot_general | solution.py:60
  277.7 3.9 convolution_convert_fusion
  282.9 3.8 collective-permute-start
  287.3 9.5 %fusion.76 = (f32[1024]{0:T(1024)S(1)}, f32[1024]{0:T(1024)S(1)}, f32[1024,512]{1,0:T(8,128)}) fusion(f32[1054,512]{1,0:T(8,128)S(1)} %maximum_convert_fusion, f32[512]{0:T(512)S(1)} %bitcast.143, f32[512]{0:T(512)S(1)} %bitcast.144, f32[512]{0:T(512)S(1)} %bitcast.146, f32[512]{0:T(512)S(1)} %bitcast.147, f32[512]{0:T(512)S(1)} %bitcast.148, ...), kind=kLoop, calls=%fused_computation.138 | loop fusion | flops 33552384 | bytes 67180544 | tf_op jit(solution)/shard_map/reduce_sum | solution.py:118
  296.8 2.5 all-reduce
  299.2 1.3 fusion.42
  302.3 1.9 fusion.3
  304.3 2.2 fusion.6
  306.7 2.4 fusion.41
  309.1 0.7 copy.46
  309.8 23.1 %all-gather.14.cloned.1.call-done = bf16[2048,512]{1,0:T(8,128)(2,1)} async-done(((bf16[128,512]{1,0:T(8,128)(2,1)}), bf16[2048,512]{1,0:T(8,128)(2,1)}) %all-gather.14.cloned.1.call-update) | async-done | bytes 2097168 | tf_op jit(solution)/shard_map/all_gather | solution.py:56
  332.9 7.4 %fusion.45 = f32[1024,2048]{1,0:T(8,128)} fusion(bf16[2048,512]{1,0:T(8,128)(2,1)} %all-gather.14.cloned.1.call-done, bf16[64,8,8,128]{3,2,1,0:T(8,128)(2,1)S(1)} %bitcast.129), kind=kOutput, calls=%fused_computation.91 | convolution fusion | flops 2147483648 | bytes 11534336 | tf_op jit(solution)/shard_map/dot_general | solution.py:126
  340.3 54.6 %all-gather.20.cloned.1.call-done = bf16[2048,512]{1,0:T(8,128)(2,1)} async-done(((bf16[128,512]{1,0:T(8,128)(2,1)}), bf16[2048,512]{1,0:T(8,128)(2,1)}) %all-gather.20.cloned.1.call-update) | async-done | bytes 2097168 | tf_op jit(solution)/shard_map/all_gather | solution.py:57
  394.9 7.3 %add_convert_fusion = bf16[1024,2048]{1,0:T(8,128)(2,1)} fusion(f32[1024,2048]{1,0:T(8,128)} %fusion.45, bf16[2048,512]{1,0:T(8,128)(2,1)} %all-gather.20.cloned.1.call-done, f32[1024,512]{1,0:T(8,128)S(1)} %copy-done, f32[512]{0:T(512)S(1)} %copy-done.32, f32[512]{0:T(512)S(1)} %copy-done.33, f32[1024]{0:T(1024)S(1)} %get-tuple-element.43, ...), kind=kOutput, calls=%fused_computation.10 | convolution fusion | flops 2156396544 | bytes 16789504 | tf_op jit(solution)/shard_map/dot_general | solution.py:130
  403.0 10.3 %reduce-scatter.2.cloned.1.call-done = bf16[512,2048]{1,0:T(8,128)(2,1)} async-done(((bf16[1024,2048]{1,0:T(8,128)(2,1)}), bf16[512,2048]{1,0:T(8,128)(2,1)}) %reduce-scatter.2.cloned.1.call-update) | async-done | bytes 2097168 | tf_op jit(solution)/shard_map/reduce_scatter | solution.py:127
  (114 shorter events, 8.3 us)
Async XLA Ops:
  7.2 18.8 %all-gather.8.cloned.1.call-start = ((), (), s32[]{:S(2)}) async-start(), calls=%async_computation.2 | async-start | bytes 6291456 | tf_op jit(solution)/shard_map/all_gather | solution.py:46
  7.9 13.5 %copy-start.5 = (f32[31,512]{1,0:T(8,128)S(1)}, f32[31,512]{1,0:T(8,128)}, u32[]{:S(2)}) copy-start(f32[31,512]{1,0:T(8,128)} %param.25) | copy-start | bytes 190468
  7.9 14.9 %copy-start.28 = (f32[8]{0:T(128)S(1)}, f32[8]{0:T(128)}, u32[]{:S(2)}) copy-start(f32[8]{0:T(128)} %param.24) | copy-start | bytes 100
  7.9 15.0 %copy-start.29 = (f32[64]{0:T(128)S(1)}, f32[64]{0:T(128)}, u32[]{:S(2)}) copy-start(f32[64]{0:T(128)} %param.23) | copy-start | bytes 772
  7.9 82.7 %all-gather.16.cloned.1.call-start = ((), (), s32[]{:S(2)}) async-start(), calls=%async_computation.6 | async-start | bytes 2228224 | tf_op jit(solution)/shard_map/all_gather | solution.py:54
  8.7 143.9 %all-gather.18.cloned.1.call-start = ((), (), s32[]{:S(2)}) async-start(), calls=%async_computation.7 | async-start | bytes 2228224 | tf_op jit(solution)/shard_map/all_gather | solution.py:55
  9.4 199.7 %all-gather.10.cloned.1.call-start = ((), (), s32[]{:S(2)}) async-start(), calls=%async_computation.3 | async-start | bytes 1114112 | tf_op jit(solution)/shard_map/all_gather | solution.py:50
  10.0 261.0 %all-gather.12.cloned.1.call-start = ((), (), s32[]{:S(2)}) async-start(), calls=%async_computation.4 | async-start | bytes 2228224 | tf_op jit(solution)/shard_map/all_gather | solution.py:49
  10.6 322.3 %all-gather.14.cloned.1.call-start = ((), (), s32[]{:S(2)}) async-start(), calls=%async_computation.5 | async-start | bytes 2228224 | tf_op jit(solution)/shard_map/all_gather | solution.py:56
  12.2 265.4 %all-to-all-start = ((bf16[16,128,256]{2,1,0:T(8,128)(2,1)}), bf16[16,128,256]{2,1,0:T(8,128)(2,1)S(1)}, u32[]{:S(2)}, u32[]{:S(2)}) async-start(bf16[16,128,256]{2,1,0:T(8,128)(2,1)} %stack.2), calls=%async_computation | async-start | bytes 2097152 | tf_op jit(solution)/shard_map/all_to_all | solution.py:52
  20.6 374.3 %all-gather.20.cloned.1.call-start = ((), (), s32[]{:S(2)}) async-start(), calls=%async_computation.8 | async-start | bytes 2228224 | tf_op jit(solution)/shard_map/all_gather | solution.py:57
  21.4 391.9 %reduce-scatter.2.cloned.1.call-start = ((), (), s32[]{:S(2)}) async-start(), calls=%async_computation.9 | async-start | bytes 6291456 | tf_op jit(solution)/shard_map/reduce_scatter | solution.py:127
  23.4 67.2 %copy-start.30 = (f32[2048]{0:T(1024)S(1)}, f32[2048]{0:T(1024)}, u32[]{:S(2)}) copy-start(f32[2048]{0:T(1024)} %param.16) | copy-start | bytes 24580
  29.0 241.9 %copy-start.26 = (f32[1024]{0:T(1024)}, f32[1024]{0:T(1024)S(1)}, u32[]{:S(2)}) copy-start(f32[1024]{0:T(1024)S(1)} %add_rsqrt_fusion.3) | copy-start | bytes 12292
  159.7 127.1 %collective-permute-start.1 = (bf16[30,512]{1,0:T(8,128)(2,1)S(1)}, bf16[30,512]{1,0:T(8,128)(2,1)S(1)}, u32[]{:S(2)}, u32[]{:S(2)}) collective-permute-start(bf16[30,512]{1,0:T(8,128)(2,1)S(1)} %slice.281), channel_id=1, source_target_pairs={{0,2},{2,4},{4,6},{6,8},{8,10},{10,12},{12,14},{14,16},{16,18},{18... | collective-permute-start | bytes 92168 | tf_op jit(solution)/shard_map/ppermute | solution.py:16
  213.3 64.4 %copy-start.31 = (f32[2048]{0:T(1024)S(1)}, f32[2048]{0:T(1024)}, u32[]{:S(2)}) copy-start(f32[2048]{0:T(1024)} %param.16) | copy-start | bytes 24580
  277.7 4.5 %copy-start.1 = (f32[1024,512]{0,1:T(8,128)S(1)}, f32[1024,512]{0,1:T(8,128)}, u32[]{:S(2)}) copy-start(f32[1024,512]{0,1:T(8,128)} %get-tuple-element.47) | copy-start | bytes 6291460
  282.3 4.5 %copy-start.3 = (bf16[1024,512]{1,0:T(8,128)(2,1)S(1)}, bf16[1024,512]{1,0:T(8,128)(2,1)}, u32[]{:S(2)}) copy-start(bf16[1024,512]{1,0:T(8,128)(2,1)} %copy-done.2) | copy-start | bytes 3145732
  282.7 4.4 %copy-start.6 = (f32[1,512]{1,0:T(1,128)S(1)}, f32[1,512]{1,0:T(1,128)}, u32[]{:S(2)}) copy-start(f32[1,512]{1,0:T(1,128)} %get-tuple-element.41) | copy-start | bytes 6148
  282.7 4.4 %copy-start.7 = (f32[1,512]{1,0:T(1,128)S(1)}, f32[1,512]{1,0:T(1,128)}, u32[]{:S(2)}) copy-start(f32[1,512]{1,0:T(1,128)} %get-tuple-element.11) | copy-start | bytes 6148
  282.8 4.4 %copy-start.8 = (f32[1,512]{1,0:T(1,128)S(1)}, f32[1,512]{1,0:T(1,128)}, u32[]{:S(2)}) copy-start(f32[1,512]{1,0:T(1,128)} %get-tuple-element.12) | copy-start | bytes 6148
  282.8 4.4 %copy-start.9 = (f32[1,512]{1,0:T(1,128)S(1)}, f32[1,512]{1,0:T(1,128)}, u32[]{:S(2)}) copy-start(f32[1,512]{1,0:T(1,128)} %get-tuple-element.13) | copy-start | bytes 6148
  282.8 4.4 %copy-start.10 = (f32[1,512]{1,0:T(1,128)S(1)}, f32[1,512]{1,0:T(1,128)}, u32[]{:S(2)}) copy-start(f32[1,512]{1,0:T(1,128)} %get-tuple-element.14) | copy-start | bytes 6148
  282.8 4.4 %copy-start.11 = (f32[1,512]{1,0:T(1,128)S(1)}, f32[1,512]{1,0:T(1,128)}, u32[]{:S(2)}) copy-start(f32[1,512]{1,0:T(1,128)} %get-tuple-element.15) | copy-start | bytes 6148
  282.8 4.4 %copy-start.12 = (f32[1,512]{1,0:T(1,128)S(1)}, f32[1,512]{1,0:T(1,128)}, u32[]{:S(2)}) copy-start(f32[1,512]{1,0:T(1,128)} %get-tuple-element.16) | copy-start | bytes 6148
  282.8 4.4 %copy-start.13 = (f32[1,512]{1,0:T(1,128)S(1)}, f32[1,512]{1,0:T(1,128)}, u32[]{:S(2)}) copy-start(f32[1,512]{1,0:T(1,128)} %get-tuple-element.17) | copy-start | bytes 6148
  282.8 4.4 %copy-start.14 = (f32[1,512]{1,0:T(1,128)S(1)}, f32[1,512]{1,0:T(1,128)}, u32[]{:S(2)}) copy-start(f32[1,512]{1,0:T(1,128)} %get-tuple-element.18) | copy-start | bytes 6148
  282.8 4.4 %copy-start.15 = (f32[1,512]{1,0:T(1,128)S(1)}, f32[1,512]{1,0:T(1,128)}, u32[]{:S(2)}) copy-start(f32[1,512]{1,0:T(1,128)} %get-tuple-element.19) | copy-start | bytes 6148
  282.9 16.3 %collective-permute-start = (bf16[128,512]{0,1:T(8,128)(2,1)}, bf16[128,512]{0,1:T(8,128)(2,1)}, u32[]{:S(2)}, u32[]{:S(2)}) collective-permute-start(bf16[128,512]{0,1:T(8,128)(2,1)} %fusion.58), channel_id=1, source_target_pairs={{0,2},{2,4},{4,6},{6,8},{8,10},{10,12},{12,14},{14,16},{16,18},{18... | collective-permute-start | bytes 393224 | tf_op jit(solution)/shard_map/ppermute | solution.py:16
  332.9 62.0 %copy-start = (f32[1024,512]{1,0:T(8,128)S(1)}, f32[1024,512]{1,0:T(8,128)}, u32[]{:S(2)}) copy-start(f32[1024,512]{1,0:T(8,128)} %get-tuple-element.6) | copy-start | bytes 6291460
  332.9 62.0 %copy-start.32 = (f32[512]{0:T(512)S(1)}, f32[512]{0:T(512)}, u32[]{:S(2)}) copy-start(f32[512]{0:T(512)} %param.27) | copy-start | bytes 6148
  332.9 62.0 %copy-start.33 = (f32[512]{0:T(512)S(1)}, f32[512]{0:T(512)}, u32[]{:S(2)}) copy-start(f32[512]{0:T(512)} %param.26) | copy-start | bytes 6148
  (13 other events, 49.3 us)
Sparse Core Ops, SparseCore 0:
  9.5 16.3 all-gather.7
  28.7 61.8 all-gather.15
  93.4 59.1 all-gather.17
  155.2 53.8 all-gather.9
  211.7 59.2 all-gather.11
  273.6 59.2 all-gather.13
  335.7 59.1 all-gather.19
  402.4 10.8 reduce-scatter.1
